TPU v7x, 32 devices: a whole 2x2x4 slice. The times are simulated.
32 devices in a mesh: grp: 2 (over y), fs: 4 (over z), tp: 4 (over x, core).
Axes of the slice: x: 2, y: 2, z: 4, core: 2. Of those that a mesh axis runs over, the one named last changes fastest.
Arguments:
- layer_input: bfloat16 [3072, 2048], P(('grp', 'fs'), 'tp'), parts along dimension 0, may hold values from -6 to 6
- first_gain: bfloat16 [1, 2048], P(None, 'tp'), may hold values from 0.099609375 to 1.8984375
- ffn_gate_w: bfloat16 [2048, 6144], P('fs', 'tp'), may hold values from -0.125 to 0.125
- ffn_up_w: bfloat16 [2048, 6144], P('fs', 'tp'), may hold values from -0.125 to 0.125
- ffn_down_w: bfloat16 [6144, 2048], P('tp', 'fs'), may hold values from -0.078125 to 0.078125
- mixer_gain: bfloat16 [1, 2048], P(None, 'tp'), may hold values from 0.099609375 to 1.8984375
- pool_in_w: bfloat16 [2048, 1024], P('fs', 'tp'), may hold values from -0.125 to 0.125
- mixer_gate_w: bfloat16 [2048, 2048], P('fs', 'tp'), may hold values from -0.125 to 0.125
- group_mix_w: bfloat16 [8, 128, 128], P('tp'), may hold values from -0.5 to 0.5
- pool_scale: float32 [1, 1024], P(None, 'tp'), may hold values from 0.1 to 1.9
- mixer_out_w: bfloat16 [1024, 2048], P('tp', 'fs'), may hold values from -0.1875 to 0.1875
- second_gain: bfloat16 [1, 2048], P(None, 'tp'), may hold values from 0.099609375 to 1.8984375
Outputs:
- layer_output: bfloat16 [3072, 2048], P(('grp', 'fs'), 'tp'), parts along dimension 0
There are 2 independent parts, one for each index of `grp`. A program takes and returns all parts, laid end to end along the dimension named above; an argument that names none is the same for every part. Nothing has to cross between parts.
All inputs are finite; a program needn't handle non-finite values.
Results may differ from a plain program's by a relative error of at most 0.015.
Values may be sent and summed in bfloat16 or wider, within the bound.
A program may use at most 64 MiB of HBM per device.

v0:
```python
import functools

import jax
import jax.numpy as jnp
from jax import lax
from jax.experimental import pallas as pl
from jax.experimental.pallas import tpu as pltpu
from jax.sharding import PartitionSpec as P

MESH = pl.DeviceIdType.MESH
F32 = jnp.float32
BF16 = jnp.bfloat16
GAIN_ROWS = 16


def ceil_pieces(rows, wanted):
    while rows % (wanted * 16) != 0:
        wanted -= 1
    return wanted


def layer_kernel(
    sizes,
    payload,
    gate_w,
    up_w,
    down_w,
    pool_w,
    mgate_w,
    mout_w,
    mix_w,
    scale_w,
    out,
    gate_all,
    up_all,
    down_all,
    pool_all,
    mgate_all,
    mout_all,
    input_all,
    value_all,
    scaled,
    factor,
    hidden,
    pooled,
    logit,
    parts,
    sums,
    local_sem,
    z_recv,
    y_recv,
    up_sem,
    low_sem,
    y_sem,
    x_send,
    x_relay,
    x_recv,
    s_send,
    s_recv,
):
    grps, planes, tps, piece_counts = sizes
    g = lax.axis_index("grp")
    f = lax.axis_index("fs")
    tp = lax.axis_index("tp")
    rows, width = out.shape
    chips = tps // 2
    chip, core = tp // 2, tp % 2
    partner = chip * 2 + (core + 1) % 2
    twins = [((chip + i) % chips) * 2 + core for i in range(1, chips)]
    crosses = [((chip + i) % chips) * 2 + (core + 1) % 2 for i in range(1, chips)]
    peers = twins + [partner]
    other_grps = [(g + d) % grps for d in range(1, grps)]

    barrier = pltpu.get_barrier_semaphore()
    for peer in peers:
        pl.semaphore_signal(barrier, inc=1, device_id={"tp": peer}, device_id_type=MESH)
    for other in other_grps:
        pl.semaphore_signal(barrier, inc=1, device_id={"grp": other}, device_id_type=MESH)

    @pl.when(f > 0)
    def _():
        pl.semaphore_signal(barrier, inc=1, device_id={"fs": f - 1}, device_id_type=MESH)

    @pl.when(f < planes - 1)
    def _():
        pl.semaphore_signal(barrier, inc=1, device_id={"fs": f + 1}, device_id_type=MESH)

    inner = jnp.where(f > 0, 1, 0) + jnp.where(f < planes - 1, 1, 0)
    pl.semaphore_wait(barrier, len(peers) + len(other_grps) + inner)

    def value_copy(phase, block, peer, relay=False):
        ref = input_all if phase == 0 else value_all.at[phase - 1]
        fresh = phase == 0 and not relay
        return pltpu.make_async_remote_copy(
            src_ref=payload if fresh else ref.at[block],
            dst_ref=ref.at[block],
            send_sem=x_relay.at[phase, block] if relay else x_send.at[phase, peer],
            recv_sem=x_recv.at[phase, block],
            device_id={"tp": peer},
            device_id_type=MESH,
        )

    def sum_copy(phase, block, slot, peer):
        return pltpu.make_async_remote_copy(
            src_ref=parts.at[phase, block],
            dst_ref=sums.at[phase, slot],
            send_sem=s_send.at[phase, block],
            recv_sem=s_recv.at[phase, slot],
            device_id={"tp": peer},
            device_id_type=MESH,
        )

    weights = (
        (gate_w, gate_all, False),
        (up_w, up_all, False),
        (down_w, down_all, True),
        (pool_w, pool_all, False),
        (mgate_w, mgate_all, False),
        (mout_w, mout_all, True),
    )
    pieces = []
    for number, (shard, whole, stacked) in enumerate(weights):
        for part in range(piece_counts[number]):
            pieces.append((number, part))

    def place(piece, plane, grp):
        number, part = pieces[piece]
        shard, whole, stacked = weights[number]
        tall = shard.shape[0]
        half = tall // grps
        size = half // piece_counts[number]
        start = grp * half + part * size
        if stacked:
            return whole.at[plane, pl.ds(pl.multiple_of(start, 16), size), :]
        return whole.at[pl.ds(pl.multiple_of(plane * tall + start, 16), size), :]

    def own_place(piece):
        number, part = pieces[piece]
        shard = weights[number][0]
        half = shard.shape[0] // grps
        size = half // piece_counts[number]
        return shard.at[pl.ds(pl.multiple_of(g * half + part * size, 16), size), :]

    def z_copy(piece, plane, step, own=False):
        spot = place(piece, plane, g)
        return pltpu.make_async_remote_copy(
            src_ref=own_place(piece) if own else spot,
            dst_ref=spot,
            send_sem=(up_sem if step > 0 else low_sem).at[piece, plane],
            recv_sem=z_recv.at[piece, plane],
            device_id={"fs": f + step},
            device_id_type=MESH,
        )

    def y_copy(piece, plane, number, source):
        spot = place(piece, plane, source)
        return pltpu.make_async_remote_copy(
            src_ref=spot,
            dst_ref=spot,
            send_sem=y_sem.at[piece, plane, number],
            recv_sem=y_recv.at[piece, plane, source],
            device_id={"grp": other_grps[number]},
            device_id_type=MESH,
        )

    def send_own(piece):

        @pl.when(f < planes - 1)
        def _():
            z_copy(piece, f, 1, own=True).start()

        @pl.when(f > 0)
        def _():
            z_copy(piece, f, -1, own=True).start()

    def pass_on(piece):
        if piece + 1 < mixer_start:
            send_own(piece + 1)
        for hop in range(1, planes):

            @pl.when(f >= hop)
            def _():
                z_copy(piece, f - hop, -1).wait_recv()

                @pl.when(f < planes - 1)
                def _():
                    z_copy(piece, f - hop, 1).start()

                for number in range(len(other_grps)):
                    y_copy(piece, f - hop, number, g).start()

            @pl.when(f + hop < planes)
            def _():
                z_copy(piece, f + hop, 1).wait_recv()

                @pl.when(f > 0)
                def _():
                    z_copy(piece, f + hop, -1).start()

                for number in range(len(other_grps)):
                    y_copy(piece, f + hop, number, g).start()

    def of(*numbers):
        return [p for p, (number, part) in enumerate(pieces) if number in numbers]

    mixer_start = of(3)[0]

    def arrive(*numbers):
        for number in numbers:
            shard, whole, stacked = weights[number]
            local_copy(number).wait()
        for piece in of(*numbers):
            for step in range(1, planes):
                plane = (f + step) % planes
                for number, other in enumerate(other_grps):
                    y_copy(piece, plane, number, other).wait_recv()

    def local_copy(number):
        shard, whole, stacked = weights[number]
        tall = shard.shape[0]
        spot = whole.at[f] if stacked else whole.at[pl.ds(pl.multiple_of(f * tall, 16), tall), :]
        return pltpu.make_async_copy(shard, spot, local_sem.at[number])

    def local_input():
        return pltpu.make_async_copy(payload, input_all.at[tp], local_sem.at[len(weights)])

    row_tile = 32

    def scale_values(phase):
        for twin in twins:
            value_copy(phase, twin, partner).wait_recv()
            value_copy(phase, twin, partner, relay=True).start()
        for block in [partner] + crosses:
            value_copy(phase, block, partner).wait_recv()
        ref = input_all if phase == 0 else value_all.at[phase - 1]

        def body(step, carry):
            span = pl.ds(pl.multiple_of(step * row_tile, row_tile), row_tile)
            total = jnp.zeros((row_tile, 1), F32)
            for t in range(tps):
                gains = input_all[t, rows : rows + GAIN_ROWS, :].astype(F32)
                value = ref[t, span, :].astype(F32)
                total = total + jnp.sum(value * value, axis=1, keepdims=True)
                scaled[span, t * width : (t + 1) * width] = (
                    value * gains[phase : phase + 1]
                ).astype(BF16)
            factor[span, :] = lax.rsqrt(total / (tps * width) + 1e-06)
            return carry

        lax.fori_loop(0, rows // row_tile, body, 0)

    def hidden_units():
        units = hidden.shape[1]
        tile = 256 if units % 256 == 0 else 128

        def body(step, carry):
            span = pl.ds(pl.multiple_of(step * tile, tile), tile)
            gate = factor[...] * jnp.dot(
                scaled[...], gate_all[:, span], preferred_element_type=F32
            )
            up = factor[...] * jnp.dot(scaled[...], up_all[:, span], preferred_element_type=F32)
            hidden[:, span] = (jax.nn.silu(gate) * up).astype(BF16)
            return carry

        lax.fori_loop(0, units // tile, body, 0)

    def project(phase, left, right_all):
        ratio = planes // tps
        block = right_all.shape[2]

        def compute(block_of):
            for piece in range(ratio):
                parts[phase, block_of, :, piece * block : (piece + 1) * block] = jnp.dot(
                    left[...], right_all[block_of * ratio + piece], preferred_element_type=F32
                ).astype(BF16)

        for twin, cross in zip(twins, crosses):
            compute(cross)
            sum_copy(phase, cross, twin, partner).start()
        for twin, cross in zip(twins, crosses):
            compute(twin)
            sum_copy(phase, cross, cross, partner).wait_recv()
            parts[phase, twin] = (
                parts[phase, twin].astype(F32) + sums[phase, cross].astype(F32)
            ).astype(BF16)
            sum_copy(phase, twin, tp, twin).start()
        compute(partner)
        sum_copy(phase, partner, tp, partner).start()
        compute(tp)

    def total_of(phase):
        total = parts[phase, tp].astype(F32)
        for peer in [partner] + twins:
            sum_copy(phase, peer, peer, partner).wait_recv()
            total = total + sums[phase, peer].astype(F32)
        return total

    def spread(phase):
        for peer in peers:
            value_copy(phase, tp, peer).start()

    local_input().start()
    spread(0)
    send_own(0)
    for number in range(len(weights)):
        local_copy(number).start()
    first_pieces = of(0, 1)
    pass_on(first_pieces[0])
    local_input().wait()
    scale_values(0)
    for piece in first_pieces[1:]:
        pass_on(piece)
    for piece in of(2)[:1]:
        pass_on(piece)
    arrive(0, 1)
    hidden_units()
    for piece in of(2)[1:]:
        pass_on(piece)
    for piece in range(mixer_start, len(pieces)):
        send_own(piece)
    arrive(2)
    project(0, hidden, down_all)

    for piece in of(3):
        pass_on(piece)
    value_all[0, tp] = (
        input_all[tp, 0:rows, :].astype(F32) + 0.5 * total_of(0)
    ).astype(BF16)
    spread(1)
    for piece in of(4):
        pass_on(piece)
    scale_values(1)
    for piece in of(5):
        pass_on(piece)
    arrive(3, 4)
    groups, group_width = mix_w.shape[0], mix_w.shape[1]
    pool_pre = (
        factor[...] * jnp.dot(scaled[...], pool_all[...], preferred_element_type=F32)
    ).astype(BF16)
    position = lax.broadcasted_iota(jnp.int32, (rows, group_width), 0)
    for group in range(groups):
        span = slice(group * group_width, (group + 1) * group_width)
        value = pool_pre[:, span].astype(F32)
        kind = (tp * groups + group) % 4
        running = value
        chosen = jnp.zeros_like(value)
        for level in range(4):
            lag = 2**level
            running = running + jnp.where(
                position >= lag, pltpu.roll(running, lag, axis=0), 0.0
            )
            counts = jnp.minimum(position + 1, 2 * lag).astype(F32)
            chosen = jnp.where(kind == level, running / counts, chosen)
        trail = (chosen - value).astype(BF16)
        mixed = jnp.dot(trail, mix_w[group], preferred_element_type=F32)
        pooled[:, span] = (mixed * scale_w[:, span]).astype(BF16)
    arrive(5)
    project(1, pooled, mout_all)
    logit[...] = factor[...] * jnp.dot(scaled[...], mgate_all[...], preferred_element_type=F32)
    value_all[1, tp] = (
        value_all[0, tp].astype(F32) + jax.nn.sigmoid(logit[...]) * total_of(1)
    ).astype(BF16)

    spread(2)
    scale_values(2)
    hidden_units()
    project(2, hidden, down_all)
    out[...] = (value_all[1, tp].astype(F32) + 0.5 * total_of(2)).astype(BF16)

    for phase in range(3):
        for peer in peers:
            value_copy(phase, tp, peer).wait_send()
        for twin in twins:
            value_copy(phase, twin, partner, relay=True).wait_send()
        for block in crosses + twins + [partner]:
            sum_copy(phase, block, tp, partner).wait_send()
    for piece in range(len(pieces)):

        @pl.when(f < planes - 1)
        def _():
            z_copy(piece, f, 1, own=True).wait_send()

        @pl.when(f > 0)
        def _():
            z_copy(piece, f, -1, own=True).wait_send()

        for hop in range(1, planes):

            @pl.when(f >= hop)
            def _():
                @pl.when(f < planes - 1)
                def _():
                    z_copy(piece, f - hop, 1).wait_send()

                for number in range(len(other_grps)):
                    y_copy(piece, f - hop, number, g).wait_send()

            @pl.when(f + hop < planes)
            def _():
                @pl.when(f > 0)
                def _():
                    z_copy(piece, f + hop, -1).wait_send()

                for number in range(len(other_grps)):
                    y_copy(piece, f + hop, number, g).wait_send()


def per_device(
    grps,
    planes,
    tps,
    layer_input,
    first_gain,
    ffn_gate_w,
    ffn_up_w,
    ffn_down_w,
    mixer_gain,
    pool_in_w,
    mixer_gate_w,
    group_mix_w,
    pool_scale,
    mixer_out_w,
    second_gain,
):
    rows, width = layer_input.shape
    features = width * tps
    gains = jnp.concatenate([first_gain, mixer_gain, second_gain], axis=0)
    payload = jnp.concatenate(
        [layer_input, jnp.pad(gains, ((0, GAIN_ROWS - 3), (0, 0)))], axis=0
    )
    units = ffn_gate_w.shape[1]
    channels = pool_in_w.shape[1]
    fine = max(16 // planes, 1)
    wanted = (fine, fine, fine, max(fine // 4, 1), max(fine // 2, 1), max(fine // 4, 1))
    shards = (ffn_gate_w, ffn_up_w, ffn_down_w, pool_in_w, mixer_gate_w, mixer_out_w)
    piece_counts = tuple(
        ceil_pieces(shard.shape[0] // grps, count) for shard, count in zip(shards, wanted)
    )
    n = sum(piece_counts)
    dma = pltpu.SemaphoreType.DMA
    whole = pl.BlockSpec(memory_space=pltpu.VMEM)
    remote = pl.BlockSpec(memory_space=pl.ANY)
    return pl.pallas_call(
        functools.partial(layer_kernel, (grps, planes, tps, piece_counts)),
        out_shape=jax.ShapeDtypeStruct((rows, width), BF16),
        in_specs=[remote] * 7 + [whole] * 2,
        out_specs=whole,
        scratch_shapes=[
            pltpu.VMEM((features, units), BF16),
            pltpu.VMEM((features, units), BF16),
            pltpu.VMEM((planes,) + ffn_down_w.shape, BF16),
            pltpu.VMEM((features, channels), BF16),
            pltpu.VMEM((features, width), BF16),
            pltpu.VMEM((planes,) + mixer_out_w.shape, BF16),
            pltpu.VMEM((tps, rows + GAIN_ROWS, width), BF16),
            pltpu.VMEM((2, tps, rows, width), BF16),
            pltpu.VMEM((rows, features), BF16),
            pltpu.VMEM((rows, 1), F32),
            pltpu.VMEM((rows, units), BF16),
            pltpu.VMEM((rows, channels), BF16),
            pltpu.VMEM((rows, width), F32),
            pltpu.VMEM((3, tps, rows, width), BF16),
            pltpu.VMEM((3, tps, rows, width), BF16),
            dma((len(shards) + 1,)),
            dma((n, planes)),
            dma((n, planes, grps)),
            dma((n, planes)),
            dma((n, planes)),
            dma((n, planes, max(grps - 1, 1))),
            dma((3, tps)),
            dma((3, tps)),
            dma((3, tps)),
            dma((3, tps)),
            dma((3, tps)),
        ],
        compiler_params=pltpu.CompilerParams(
            collective_id=0, has_side_effects=True, vmem_limit_bytes=60 * 1024 * 1024
        ),
    )(payload, *shards, group_mix_w, pool_scale)


def solution(mesh):
    return jax.shard_map(
        functools.partial(
            per_device, mesh.shape["grp"], mesh.shape["fs"], mesh.shape["tp"]
        ),
        mesh=mesh,
        in_specs=(
            P(("grp", "fs"), "tp"),
            P(None, "tp"),
            P("fs", "tp"),
            P("fs", "tp"),
            P("tp", "fs"),
            P(None, "tp"),
            P("fs", "tp"),
            P("fs", "tp"),
            P("tp", None, None),
            P(None, "tp"),
            P("tp", "fs"),
            P(None, "tp"),
        ),
        out_specs=P(("grp", "fs"), "tp"),
        check_vma=False,
    )
```

profile of v0, /device:TPU:0, one launch (start us, length us, event | category | flops | bytes accessed | tf_op | source)
XLA Modules:
  0.0 266.1 jit_solution(8543862485681216470)
XLA Ops:
  0.0 0.7 fusion.4
  0.7 1.8 pad_maximum_fusion.payload
  2.5 261.8 %shard_map.118 = bf16[384,512]{1,0:T(8,128)(2,1)} custom-call(bf16[400,512]{1,0:T(8,128)(2,1)} %pad_maximum_fusion.payload, bf16[512,1536]{1,0:T(8,128)(2,1)} %gate_w.1, bf16[512,1536]{1,0:T(8,128)(2,1)} %up_w.1, bf16[1536,512]{1,0:T(8,128)(2,1)} %down_w.1, bf16[512,256]{1,0:T(8,128)(2,1)} %pool_w.1, bf16[512,512]{1,0:T(8,128)(2,1)} %mgate_w.1, ...), custom_call_target="tpu_custom_call" | custom-call | tf_op jit(solution)/shard_map/pallas_call | solution.py:443
  264.3 1.8 copy.14
where the time goes:
time: 266 us
  Pallas kernels  262 us (98%)
    pallas_call x1, Pallas kernels, per_device(): pl.pallas_call(functools.partial(layer_kernel, (grps, planes, tps, piece_...  262 us

commit v1 on v0

v1 whole, which is shorter than its diff:
```python
import functools

import jax
import jax.numpy as jnp
from jax import lax
from jax.experimental import pallas as pl
from jax.experimental.pallas import tpu as pltpu
from jax.sharding import PartitionSpec as P

MESH = pl.DeviceIdType.MESH
F32 = jnp.float32
BF16 = jnp.bfloat16
scope = jax.named_scope
GAIN_ROWS = 16


def ceil_pieces(rows, wanted):
    while rows % (wanted * 16) != 0:
        wanted -= 1
    return wanted


def layer_kernel(
    sizes,
    inputs,
    gain_rows,
    gate_w,
    up_w,
    down_w,
    pool_w,
    mgate_w,
    mout_w,
    mix_w,
    scale_w,
    out,
    gate_all,
    up_all,
    down_all,
    pool_all,
    mgate_all,
    mout_all,
    input_all,
    gain_all,
    value_all,
    scaled,
    factor,
    hidden,
    pooled,
    logit,
    parts,
    sums,
    mate_out,
    mate_in,
    mate_top,
    local_sem,
    z_recv,
    y_recv,
    z_send,
    y_send,
    v_send,
    v_relay,
    v_recv,
    g_send,
    g_relay,
    g_recv,
    s_send,
    s_recv,
    m_send,
    m_recv,
):
    grps, planes, tps, mates, piece_counts = sizes
    g = lax.axis_index("grp")
    f = lax.axis_index("fs")
    tp = lax.axis_index("tp")
    rows, width = out.shape
    chips = tps // 2
    chip, core = tp // 2, tp % 2
    partner = chip * 2 + (core + 1) % 2
    twins = [((chip + i) % chips) * 2 + core for i in range(1, chips)]
    crosses = [((chip + i) % chips) * 2 + (core + 1) % 2 for i in range(1, chips)]
    peers = twins + [partner]
    other_grps = [(g + d) % grps for d in range(1, grps)]
    side = f % mates
    mate = f + 1 - 2 * side

    barrier = pltpu.get_barrier_semaphore()
    for peer in peers:
        pl.semaphore_signal(barrier, inc=1, device_id={"tp": peer}, device_id_type=MESH)
    for other in other_grps:
        pl.semaphore_signal(barrier, inc=1, device_id={"grp": other}, device_id_type=MESH)

    @pl.when(f > 0)
    def _():
        pl.semaphore_signal(barrier, inc=1, device_id={"fs": f - 1}, device_id_type=MESH)

    @pl.when(f < planes - 1)
    def _():
        pl.semaphore_signal(barrier, inc=1, device_id={"fs": f + 1}, device_id_type=MESH)

    inner = jnp.where(f > 0, 1, 0) + jnp.where(f < planes - 1, 1, 0)
    pl.semaphore_wait(barrier, len(peers) + len(other_grps) + inner)

    def gathered(lane):
        return input_all if lane == 0 else value_all.at[lane - 1]

    half_rows = rows // 2
    halves = (slice(0, half_rows), slice(half_rows, rows))

    def value_copy(lane, block, half, peer=None, source=None):
        relay = source is not None
        ref = inputs if lane == 0 and not relay else gathered(source if relay else lane).at[block]
        target = 1 if peer is None else 0
        if relay:
            send_sem = v_relay.at[lane, half, block, target]
        else:
            send_sem = v_send.at[lane, half, tps if peer is None else peer]
        to = lane if peer is not None else lane + 3 if lane == 0 else 4
        return pltpu.make_async_remote_copy(
            src_ref=ref.at[halves[half], :],
            dst_ref=gathered(to).at[block, halves[half], :],
            send_sem=send_sem,
            recv_sem=v_recv.at[to, half, block],
            device_id={"fs": mate} if peer is None else {"tp": peer},
            device_id_type=MESH,
        )

    def gain_copy(block, peer, relay=False):
        return pltpu.make_async_remote_copy(
            src_ref=gain_all.at[block] if relay else gain_rows,
            dst_ref=gain_all.at[block],
            send_sem=g_relay.at[block] if relay else g_send.at[peer],
            recv_sem=g_recv.at[block],
            device_id={"tp": peer},
            device_id_type=MESH,
        )

    def mate_sum_copy(ffn, block, top=False):
        if top:
            source, target = mate_out.at[ffn, halves[0], :], mate_top.at[ffn]
        else:
            target = mate_in.at[ffn, block]
            source = parts.at[ffn_lanes(ffn)[-1], block, halves[1], :]
        number = tps if top else block
        return pltpu.make_async_remote_copy(
            src_ref=source,
            dst_ref=target,
            send_sem=m_send.at[ffn, number],
            recv_sem=m_recv.at[ffn, number],
            device_id={"fs": mate},
            device_id_type=MESH,
        )

    def own_sum_copy(ffn):
        return pltpu.make_async_remote_copy(
            src_ref=mate_out.at[ffn, halves[1], :],
            dst_ref=mate_in.at[ffn, tp],
            send_sem=m_send.at[ffn, tp],
            recv_sem=m_recv.at[ffn, tp],
            device_id={"fs": mate},
            device_id_type=MESH,
        )

    def sum_copy(lane, block, slot, peer, half=None):
        span = slice(0, rows) if half is None else halves[half]
        number = 0 if half is None else half
        return pltpu.make_async_remote_copy(
            src_ref=parts.at[lane, block, span, :],
            dst_ref=sums.at[lane, slot, span, :],
            send_sem=s_send.at[lane, number, block],
            recv_sem=s_recv.at[lane, number, slot],
            device_id={"tp": peer},
            device_id_type=MESH,
        )

    weights = (
        (gate_w, gate_all, "columns"),
        (up_w, up_all, "columns"),
        (down_w, down_all, "rows"),
        (pool_w, pool_all, "plain"),
        (mgate_w, mgate_all, "plain"),
        (mout_w, mout_all, "stacked"),
    )
    pieces = []
    for numbers in ((0, 1), (2,), (3,), (4,), (5,)):
        for part in range(piece_counts[numbers[0]]):
            for number in numbers:
                for share in range(mates) if number < 3 else (None,):
                    pieces.append((number, share, part))
    share_units = down_w.shape[0] // mates

    def span_of(piece, grp):
        number, share, part = pieces[piece]
        kind = weights[number][2]
        tall = share_units if kind == "rows" else weights[number][0].shape[0]
        half = tall // grps
        size = half // piece_counts[number]
        offset = share * share_units if kind == "rows" else 0
        return offset + grp * half + part * size, size

    def place(piece, plane, grp):
        number, share, part = pieces[piece]
        shard, whole, kind = weights[number]
        start, size = span_of(piece, grp)
        if kind in ("rows", "stacked"):
            return whole.at[plane, pl.ds(pl.multiple_of(start, 16), size), :]
        span = pl.ds(pl.multiple_of(plane * shard.shape[0] + start, 16), size)
        if kind == "columns":
            return whole.at[share, span, :]
        return whole.at[span, :]

    def own_place(piece):
        number, share, part = pieces[piece]
        shard, whole, kind = weights[number]
        start, size = span_of(piece, g)
        span = pl.ds(pl.multiple_of(start, 16), size)
        if kind == "columns":
            return shard.at[span, share * share_units : (share + 1) * share_units]
        return shard.at[span, :]

    def ends(piece):
        share = pieces[piece][1]
        if share is None:
            return 0, planes - 1
        return share, planes - mates + share

    def wanted(piece):
        share = pieces[piece][1]
        return True if share is None else side == share

    def z_copy(piece, plane, step, own=False):
        spot = place(piece, plane, g)
        return pltpu.make_async_remote_copy(
            src_ref=own_place(piece) if own else spot,
            dst_ref=spot,
            send_sem=z_send.at[piece, planes if own and step < 0 else plane],
            recv_sem=z_recv.at[piece, plane],
            device_id={"fs": f + step},
            device_id_type=MESH,
        )

    def y_copy(piece, plane, number, source, arriving=False):
        spot = place(piece, plane, source)
        there = number if arriving else grps - 2 - number
        return pltpu.make_async_remote_copy(
            src_ref=spot,
            dst_ref=spot,
            send_sem=y_send.at[piece, plane, number],
            recv_sem=y_recv.at[piece, plane, there],
            device_id={"grp": other_grps[number]},
            device_id_type=MESH,
        )

    def send_own(piece, early=None):
        low, high = ends(piece)
        up, down = f < high, f > low
        if pieces[piece][0] > 2:
            outward_up, outward_down = f >= planes // 2, f < planes // 2
            up = up & (outward_up if early else jnp.logical_not(outward_up))
            down = down & (outward_down if early else jnp.logical_not(outward_down))

        @pl.when(up)
        def _():
            z_copy(piece, f, 1, own=True).start()

        @pl.when(down)
        def _():
            z_copy(piece, f, -1, own=True).start()

    def take(piece, hop):
        low, high = ends(piece)

        @pl.when((f >= hop) & (f <= high))
        def _():
            z_copy(piece, f - hop, -1).wait_recv()

            @pl.when(f < high)
            def _():
                z_copy(piece, f - hop, 1).start()

            @pl.when(wanted(piece))
            def _():
                for number in range(len(other_grps)):
                    y_copy(piece, f - hop, number, g).start()

        @pl.when((f + hop < planes) & (f >= low))
        def _():
            z_copy(piece, f + hop, 1).wait_recv()

            @pl.when(f > low)
            def _():
                z_copy(piece, f + hop, -1).start()

            @pl.when(wanted(piece))
            def _():
                for number in range(len(other_grps)):
                    y_copy(piece, f + hop, number, g).start()

    def advance(until):
        while clock[0] < until:
            step = clock[0]
            if step + ahead < len(pieces):
                send_own(step + ahead)
            if step in early_at:
                send_own(early_at[step], early=True)
            for hop in range(planes - 1, 0, -1):
                piece = step - (hop - 1) * lag
                if 0 <= piece < len(pieces):
                    take(piece, hop)
            clock[0] += 1

    def after(piece):
        return piece + 1 + (planes - 2) * lag

    def sent(piece):
        low, high = ends(piece)

        @pl.when(f < high)
        def _():
            z_copy(piece, f, 1, own=True).wait_send()

        @pl.when(f > low)
        def _():
            z_copy(piece, f, -1, own=True).wait_send()

        for hop in range(1, planes):

            @pl.when((f >= hop) & (f <= high))
            def _():
                @pl.when(f < high)
                def _():
                    z_copy(piece, f - hop, 1).wait_send()

                @pl.when(wanted(piece))
                def _():
                    for number in range(len(other_grps)):
                        y_copy(piece, f - hop, number, g).wait_send()

            @pl.when((f + hop < planes) & (f >= low))
            def _():
                @pl.when(f > low)
                def _():
                    z_copy(piece, f + hop, -1).wait_send()

                @pl.when(wanted(piece))
                def _():
                    for number in range(len(other_grps)):
                        y_copy(piece, f + hop, number, g).wait_send()

    def of(*numbers):
        return [p for p, piece in enumerate(pieces) if piece[0] in numbers]

    clock = [0]
    ahead = 3
    mixer_pieces = of(3, 4, 5)
    early_at = {8 * mixer_pieces[0] // 24 + i: p for i, p in enumerate(mixer_pieces)}
    lag = 1

    def arrive(*numbers):
        for number in numbers:
            local_copy(number).wait()
        for piece in of(*numbers):

            @pl.when(wanted(piece))
            def _():
                for step in range(1, planes):
                    plane = (f + step) % planes
                    for number, other in enumerate(other_grps):
                        y_copy(piece, plane, number, other, arriving=True).wait_recv()

    def local_copy(number):
        shard, whole, kind = weights[number]
        tall = shard.shape[0]
        span = pl.ds(pl.multiple_of(f * tall, 16), tall)
        if kind == "columns":
            mine = pl.ds(pl.multiple_of(side * share_units, 128), share_units)
            shard, spot = shard.at[:, mine], whole.at[side, span, :]
        elif kind == "rows":
            mine = pl.ds(pl.multiple_of(side * share_units, 16), share_units)
            shard, spot = shard.at[mine, :], whole.at[f, mine, :]
        elif kind == "stacked":
            spot = whole.at[f]
        else:
            spot = whole.at[span, :]
        return pltpu.make_async_copy(shard, spot, local_sem.at[number])

    def local_input():
        return pltpu.make_async_copy(inputs, input_all.at[tp], local_sem.at[len(weights)])

    def local_gain():
        return pltpu.make_async_copy(gain_rows, gain_all.at[tp], local_sem.at[len(weights) + 1])

    row_tile = [t for t in (96, 64, 32, 16) if rows % t == 0][0]

    def spread(lane, half, with_mate=False):
        for peer in peers:
            value_copy(lane, tp, half, peer).start()
        if with_mate and mates > 1:
            value_copy(lane, tp, half).start()

    def landed(lane, block, half):
        value_copy(lane, block, half, partner).wait_recv()

    def relay_values(lane, half, with_mate=False):
        for twin in twins:
            landed(lane, twin, half)
            value_copy(lane, twin, half, partner, source=lane).start()
            if with_mate and mates > 1 and half == 1:
                value_copy(lane, twin, half, source=lane).start()

    def relay_mate(lane, half):
        landed(lane, tp, half)
        for peer in peers if half == 0 else [partner]:
            value_copy(lane, tp, half, peer, source=lane).start()

    def relay_mate_twins(lane):
        for half in range(2):
            for twin in twins:
                landed(lane, twin, half)
                value_copy(lane, twin, half, partner, source=lane).start()

    def gather_start(lane):
        for half in range(2):
            spread(lane, half, with_mate=True)

    def gather_relay(lane, mate_lane):
        relay_values(lane, 0)
        if mates > 1:
            relay_mate(mate_lane, 0)
        relay_values(lane, 1, with_mate=True)
        if mates > 1:
            relay_mate(mate_lane, 1)

    def value_sent(lane, with_mate=False):
        for half in range(2):
            for peer in peers:
                value_copy(lane, tp, half, peer).wait_send()
            for twin in twins:
                value_copy(lane, twin, half, partner, source=lane).wait_send()
            if with_mate and mates > 1:
                value_copy(lane, tp, half).wait_send()
                if half == 1:
                    for twin in twins:
                        value_copy(lane, twin, half, source=lane).wait_send()

    def mate_sent(lane):
        for half in range(2):
            for peer in peers if half == 0 else [partner]:
                value_copy(lane, tp, half, peer, source=lane).wait_send()
            for twin in twins:
                value_copy(lane, twin, half, partner, source=lane).wait_send()

    def scale_values(lane, slot, gain):
        for half in range(2):
            for block in [partner] + crosses:
                landed(lane, block, half)
        ref = gathered(lane)

        def body(step, carry):
            start = pl.multiple_of(step * row_tile, row_tile)
            span = pl.ds(start, row_tile)
            target = pl.ds(slot * rows + start, row_tile)
            total = jnp.zeros((row_tile, 1), F32)
            for t in range(tps):
                gains = gain_all[t].astype(F32)
                value = ref[t, span, :].astype(F32)
                total = total + jnp.sum(value * value, axis=1, keepdims=True)
                scaled[target, t * width : (t + 1) * width] = (
                    value * gains[gain : gain + 1]
                ).astype(BF16)
            factor[target, :] = lax.rsqrt(total / (tps * width) + 1e-06)
            return carry

        lax.fori_loop(0, rows // row_tile, body, 0)

    def hidden_units(slot):
        units = hidden.shape[1]
        tile = 256 if units % 256 == 0 else 128
        mine = slice(slot * rows, (slot + 1) * rows)

        def body(step, carry):
            span = pl.ds(pl.multiple_of(step * tile, tile), tile)
            gate = factor[mine, :] * jnp.dot(
                scaled[mine, :], gate_all[side, :, span], preferred_element_type=F32
            )
            up = factor[mine, :] * jnp.dot(
                scaled[mine, :], up_all[side, :, span], preferred_element_type=F32
            )
            hidden[mine, span] = (jax.nn.silu(gate) * up).astype(BF16)
            return carry

        lax.fori_loop(0, units // tile, body, 0)

    ratio = planes // tps
    block_width = width // ratio

    def product(left, right_of, lane, slot, block_of):
        for piece in range(ratio):
            parts[lane, block_of, :, piece * block_width : (piece + 1) * block_width] = jnp.dot(
                left[slot * rows : (slot + 1) * rows, :],
                right_of(block_of * ratio + piece),
                preferred_element_type=F32,
            ).astype(BF16)

    def join_cross(lane, twin, cross):
        sum_copy(lane, cross, cross, partner).wait_recv()
        parts[lane, twin] = (
            parts[lane, twin].astype(F32) + sums[lane, cross].astype(F32)
        ).astype(BF16)

    def project_mixer(lane):
        left, right_of = pooled, lambda plane: mout_all[plane]
        for twin, cross in zip(twins, crosses):
            product(left, right_of, lane, 0, cross)
            sum_copy(lane, cross, twin, partner).start()
        for twin, cross in zip(twins, crosses):
            product(left, right_of, lane, 0, twin)
            join_cross(lane, twin, cross)
            for half in range(2):
                sum_copy(lane, twin, tp, twin, half).start()
        product(left, right_of, lane, 0, partner)
        sum_copy(lane, partner, tp, partner).start()
        product(left, right_of, lane, 0, tp)

    def sum_sent(lane, half_only=None):
        for block in crosses + [partner]:
            sum_copy(lane, block, tp, partner).wait_send()
        for twin in twins:
            for half in range(2) if half_only is None else [half_only]:
                sum_copy(lane, twin, tp, twin, half).wait_send()

    def down_of(plane):
        return down_all[plane, pl.ds(pl.multiple_of(side * share_units, 16), share_units), :]

    def ffn_lanes(ffn):
        return [ffn * (mates + 1) + slot for slot in range(mates)]

    def project_ffn(ffn):
        lanes = ffn_lanes(ffn)
        order = range(mates - 1, -1, -1)
        for slot in order:
            for twin, cross in zip(twins, crosses):
                product(hidden, down_of, lanes[slot], slot, cross)
                sum_copy(lanes[slot], cross, twin, partner).start()
        for slot in order:
            for twin, cross in zip(twins, crosses):
                product(hidden, down_of, lanes[slot], slot, twin)
                join_cross(lanes[slot], twin, cross)
                if slot > 0:
                    mate_sum_copy(ffn, twin).start()
                sum_copy(lanes[slot], twin, tp, twin, 0).start()
                if mates == 1:
                    sum_copy(lanes[slot], twin, tp, twin, 1).start()
        for slot in order:
            product(hidden, down_of, lanes[slot], slot, partner)
            sum_copy(lanes[slot], partner, tp, partner).start()
        for slot in order:
            product(hidden, down_of, lanes[slot], slot, tp)

    def half_total(lane, half, joined=False):
        total = parts[lane, tp, halves[half], :].astype(F32)
        if not joined:
            total = total + sums[lane, partner, halves[half], :].astype(F32)
        return total

    def add_twins(lane, half, total):
        for twin in twins:
            sum_copy(lane, twin, twin, partner, half).wait_recv()
            total = total + sums[lane, twin, halves[half], :].astype(F32)
        return total

    def exchange_ffn(ffn):
        lanes = ffn_lanes(ffn)
        if mates > 1:
            sum_copy(lanes[1], partner, partner, partner).wait_recv()
            mate_out[ffn, halves[1], :] = half_total(lanes[1], 1).astype(BF16)
            own_sum_copy(ffn).start()
            for twin in twins:
                mate_sum_copy(ffn, twin).wait_recv()
                parts[lanes[0], twin, halves[1], :] = (
                    parts[lanes[0], twin, halves[1], :].astype(F32)
                    + mate_in[ffn, twin].astype(F32)
                ).astype(BF16)
                sum_copy(lanes[0], twin, tp, twin, 1).start()
            mate_out[ffn, halves[0], :] = add_twins(
                lanes[1], 0, half_total(lanes[1], 0)
            ).astype(BF16)
            mate_sum_copy(ffn, tp, top=True).start()
        sum_copy(lanes[0], partner, partner, partner).wait_recv()

    def ffn_total(ffn, half):
        lane = ffn_lanes(ffn)[0]
        total = add_twins(lane, half, half_total(lane, half))
        if mates > 1 and half == 0:
            mate_sum_copy(ffn, tp, top=True).wait_recv()
            total = total + mate_top[ffn].astype(F32)
        elif mates > 1:
            own_sum_copy(ffn).wait_recv()
            total = total + mate_in[ffn, tp].astype(F32)
        return total

    def ffn_sent(ffn):
        lanes = ffn_lanes(ffn)
        sum_sent(lanes[0])
        if mates > 1:
            sum_sent(lanes[1], half_only=0)
            own_sum_copy(ffn).wait_send()
            mate_sum_copy(ffn, tp, top=True).wait_send()
            for twin in twins:
                mate_sum_copy(ffn, twin).wait_send()

    local_input().start()
    local_gain().start()
    for half in range(2):
        spread(0, half)
    for peer in peers:
        gain_copy(tp, peer).start()
    for piece in range(ahead):
        send_own(piece)
    for number in range(len(weights)):
        local_copy(number).start()
    with scope("begin"):
        advance(1)
    local_input().wait()
    local_gain().wait()
    with scope("input_own"):
        for twin in twins:
            gain_copy(twin, partner).wait_recv()
            gain_copy(twin, partner, relay=True).start()
        for block in [partner] + crosses:
            gain_copy(block, partner).wait_recv()
        for half in range(2):
            relay_values(0, half)
        scale_values(0, 0, 0)
    with scope("early"):
        if mates > 1:
            value_copy(0, tp, 0).start()
        advance(2)
        if mates > 1:
            value_copy(0, tp, 1).start()
        advance(4)
    with scope("input_mate"):
        if mates > 1:
            for twin in twins:
                value_copy(0, twin, 1, source=0).start()
            relay_mate(3, 0)
            relay_mate(3, 1)
        advance(6)
        if mates > 1:
            relay_mate_twins(3)
    with scope("early2"):
        advance(7)
    with scope("mate_scale"):
        if mates > 1:
            scale_values(3, 1, 0)
    first_last, down_last = of(0, 1)[-1], of(2)[-1]
    with scope("gate_up"):
        advance(after(first_last) + 2)
    with scope("gate_up_y"):
        arrive(0, 1)
    for slot in range(mates):
        with scope(f"hidden{slot}"):
            hidden_units(slot)
        with scope(f"step{slot}"):
            advance(min(clock[0] + 2, after(down_last)))
    with scope("down"):
        advance(after(down_last))
    with scope("down_y"):
        arrive(2)
    with scope("project0"):
        project_ffn(0)
    with scope("mix_pool"):
        advance(after(of(3)[-1]))
    with scope("exchange0"):
        exchange_ffn(0)
    with scope("mix_gate"):
        advance(after(of(4)[0]))
    with scope("first"):
        for half, span in enumerate(halves):
            value_all[0, tp, span, :] = (
                input_all[tp, span, :].astype(F32) + 0.5 * ffn_total(0, half)
            ).astype(BF16)
            spread(1, half)
    with scope("mix_rest"):
        advance(after(len(pieces) - 1))
    with scope("sent1"):
        value_sent(0, with_mate=True)
        for peer in peers:
            gain_copy(tp, peer).wait_send()
        for twin in twins:
            gain_copy(twin, partner, relay=True).wait_send()
        if mates > 1:
            mate_sent(3)
        for piece in of(0):
            sent(piece)
    with scope("relay1"):
        for half in range(2):
            relay_values(1, half)
    with scope("scale1"):
        scale_values(1, 0, 1)
    with scope("mix_y"):
        arrive(3, 4)
    groups, group_width = mix_w.shape[0], mix_w.shape[1]
    with scope("pool"):
        mixed_rows = slice(0, rows)
        pool_pre = (
            factor[mixed_rows, :]
            * jnp.dot(scaled[mixed_rows, :], pool_all[...], preferred_element_type=F32)
        ).astype(BF16)
        position = lax.broadcasted_iota(jnp.int32, (rows, group_width), 0)
        for group in range(groups):
            span = slice(group * group_width, (group + 1) * group_width)
            value = pool_pre[:, span].astype(F32)
            kind = (tp * groups + group) % 4
            running = value
            chosen = jnp.zeros_like(value)
            for level in range(4):
                lag = 2**level
                running = running + jnp.where(
                    position >= lag, pltpu.roll(running, lag, axis=0), 0.0
                )
                counts = jnp.minimum(position + 1, 2 * lag).astype(F32)
                chosen = jnp.where(kind == level, running / counts, chosen)
            trail = (chosen - value).astype(BF16)
            mixed = jnp.dot(trail, mix_w[group], preferred_element_type=F32)
            pooled[:, span] = (mixed * scale_w[:, span]).astype(BF16)
    with scope("mix_y2"):
        arrive(5)
    with scope("project1"):
        project_mixer(mates)
    with scope("logit"):
        logit[...] = factor[mixed_rows, :] * jnp.dot(
            scaled[mixed_rows, :], mgate_all[...], preferred_element_type=F32
        )
        logit[...] = jax.nn.sigmoid(logit[...])
    with scope("sent2"):
        ffn_sent(0)
        value_sent(1)
    with scope("second"):
        sum_copy(mates, partner, partner, partner).wait_recv()
        for half, span in enumerate(halves):
            value_all[1, tp, span, :] = (
                value_all[0, tp, span, :].astype(F32)
                + logit[span, :] * add_twins(mates, half, half_total(mates, half))
            ).astype(BF16)
            spread(2, half, with_mate=True)
    with scope("sent3"):
        for piece in of(1, 2):
            sent(piece)
    with scope("relay2"):
        gather_relay(2, 4)
    with scope("scale2"):
        scale_values(2, 0, 2)
    with scope("hidden2_0"):
        hidden_units(0)
    if mates > 1:
        with scope("relay4"):
            relay_mate_twins(4)
            for piece in of(3, 4, 5):
                sent(piece)
        with scope("scale4"):
            scale_values(4, 1, 2)
        with scope("hidden2_1"):
            hidden_units(1)
    with scope("project2"):
        project_ffn(1)
    with scope("exchange2"):
        exchange_ffn(1)
    with scope("sent4"):
        sum_sent(mates)
        value_sent(2, with_mate=True)
        if mates > 1:
            mate_sent(4)
        else:
            for piece in of(3, 4, 5):
                sent(piece)
    with scope("final"):
        for half, span in enumerate(halves):
            out[span, :] = (
                value_all[1, tp, span, :].astype(F32) + 0.5 * ffn_total(1, half)
            ).astype(BF16)
    with scope("sent5"):
        ffn_sent(1)


def per_device(
    grps,
    planes,
    tps,
    layer_input,
    first_gain,
    ffn_gate_w,
    ffn_up_w,
    ffn_down_w,
    mixer_gain,
    pool_in_w,
    mixer_gate_w,
    group_mix_w,
    pool_scale,
    mixer_out_w,
    second_gain,
):
    rows, width = layer_input.shape
    features = width * tps
    gains = jnp.concatenate([first_gain, mixer_gain, second_gain], axis=0)
    gain_rows = jnp.pad(gains, ((0, GAIN_ROWS - 3), (0, 0)))
    units = ffn_gate_w.shape[1]
    channels = pool_in_w.shape[1]
    mates = 2 if planes % 2 == 0 else 1
    fine = max(8 // planes, 1)
    wanted = (fine, fine, fine, max(fine // 2, 1), fine, max(fine // 2, 1))
    shards = (ffn_gate_w, ffn_up_w, ffn_down_w, pool_in_w, mixer_gate_w, mixer_out_w)
    talls = [shard.shape[0] // grps for shard in shards]
    talls[2] //= mates
    piece_counts = tuple(ceil_pieces(tall, count) for tall, count in zip(talls, wanted))
    n = mates * sum(piece_counts[:3]) + sum(piece_counts[3:])
    lanes = 2 * mates + 1
    dma = pltpu.SemaphoreType.DMA
    whole = pl.BlockSpec(memory_space=pltpu.VMEM)
    remote = pl.BlockSpec(memory_space=pl.ANY)
    return pl.pallas_call(
        functools.partial(layer_kernel, (grps, planes, tps, mates, piece_counts)),
        out_shape=jax.ShapeDtypeStruct((rows, width), BF16),
        in_specs=[remote] * 8 + [whole] * 2,
        out_specs=whole,
        scratch_shapes=[
            pltpu.VMEM((mates, features, units // mates), BF16),
            pltpu.VMEM((mates, features, units // mates), BF16),
            pltpu.VMEM((planes,) + ffn_down_w.shape, BF16),
            pltpu.VMEM((features, channels), BF16),
            pltpu.VMEM((features, width), BF16),
            pltpu.VMEM((planes,) + mixer_out_w.shape, BF16),
            pltpu.VMEM((tps, rows, width), BF16),
            pltpu.VMEM((tps, GAIN_ROWS, width), BF16),
            pltpu.VMEM((2 * mates, tps, rows, width), BF16),
            pltpu.VMEM((mates * rows, features), BF16),
            pltpu.VMEM((mates * rows, 1), F32),
            pltpu.VMEM((mates * rows, units // mates), BF16),
            pltpu.VMEM((rows, channels), BF16),
            pltpu.VMEM((rows, width), F32),
            pltpu.VMEM((lanes, tps, rows, width), BF16),
            pltpu.VMEM((lanes, tps, rows, width), BF16),
            pltpu.VMEM((2, rows, width), BF16),
            pltpu.VMEM((2, tps, rows // 2, width), BF16),
            pltpu.VMEM((2, rows // 2, width), BF16),
            dma((len(shards) + 2,)),
            dma((n, planes)),
            dma((n, planes, max(grps - 1, 1))),
            dma((n, planes + 1)),
            dma((n, planes, max(grps - 1, 1))),
            dma((5, 2, tps + 1)),
            dma((5, 2, tps, 2)),
            dma((5, 2, tps)),
            dma((tps,)),
            dma((tps,)),
            dma((tps,)),
            dma((lanes, 2, tps)),
            dma((lanes, 2, tps)),
            dma((2, tps + 1)),
            dma((2, tps + 1)),
        ],
        compiler_params=pltpu.CompilerParams(
            collective_id=0, has_side_effects=True, vmem_limit_bytes=60 * 1024 * 1024
        ),
    )(layer_input, gain_rows, *shards, group_mix_w, pool_scale)


def solution(mesh):
    return jax.shard_map(
        functools.partial(
            per_device, mesh.shape["grp"], mesh.shape["fs"], mesh.shape["tp"]
        ),
        mesh=mesh,
        in_specs=(
            P(("grp", "fs"), "tp"),
            P(None, "tp"),
            P("fs", "tp"),
            P("fs", "tp"),
            P("tp", "fs"),
            P(None, "tp"),
            P("fs", "tp"),
            P("fs", "tp"),
            P("tp", None, None),
            P(None, "tp"),
            P("tp", "fs"),
            P(None, "tp"),
        ),
        out_specs=P(("grp", "fs"), "tp"),
        check_vma=False,
    )
```

time: 266 us -> 220 us (0.83)
  Pallas kernels: 262 us -> 216 us
    pallas_call x1, Pallas kernels: 262 us -> 216 us  [per_device(): pl.pallas_call(functools.partial(layer_kernel, (grps, planes, tps, mates,...]
where the time goes in v1:
time: 220 us; the launch traced here: 219 us
  Pallas kernels  216 us (98%)
    pallas_call x1, Pallas kernels, per_device(): pl.pallas_call(functools.partial(layer_kernel, (grps, planes, tps, mates,...  216 us

profile of v1, /device:TPU:0, one launch (start us, length us, event | category | flops | bytes accessed | tf_op | source)
XLA Modules:
  0.0 219.4 jit_solution(14973008265984012789)
XLA Ops:
  0.0 1.3 fusion.4.gain_rows
  1.3 216.3 %shard_map.118 = bf16[384,512]{1,0:T(8,128)(2,1)} custom-call(bf16[384,512]{1,0:T(8,128)(2,1)} %inputs.1, bf16[16,512]{1,0:T(8,128)(2,1)} %fusion.4.gain_rows, bf16[512,1536]{1,0:T(8,128)(2,1)} %gate_w.1, bf16[512,1536]{1,0:T(8,128)(2,1)} %up_w.1, bf16[1536,512]{1,0:T(8,128)(2,1)} %down_w.1, bf16[512,256]{1,0:T(8,128)(2,1)} %pool_w.1, ...), custom_call_target="tpu_custom_call" | custom-call | tf_op jit(solution)/shard_map/pallas_call | solution.py:820
  217.7 1.8 copy.14

commit v2 on v1

--- a/solution.py
+++ b/solution.py
@@ -23,7 +23,9 @@
 def layer_kernel(
     sizes,
     inputs,
-    gain_rows,
+    first_gain,
+    mixer_gain,
+    second_gain,
     gate_w,
     up_w,
     down_w,
@@ -61,7 +63,6 @@
     v_relay,
     v_recv,
     g_send,
-    g_relay,
     g_recv,
     s_send,
     s_recv,
@@ -109,16 +110,11 @@
     def value_copy(lane, block, half, peer=None, source=None):
         relay = source is not None
         ref = inputs if lane == 0 and not relay else gathered(source if relay else lane).at[block]
-        target = 1 if peer is None else 0
-        if relay:
-            send_sem = v_relay.at[lane, half, block, target]
-        else:
-            send_sem = v_send.at[lane, half, tps if peer is None else peer]
         to = lane if peer is not None else lane + 3 if lane == 0 else 4
         return pltpu.make_async_remote_copy(
             src_ref=ref.at[halves[half], :],
             dst_ref=gathered(to).at[block, halves[half], :],
-            send_sem=send_sem,
+            send_sem=(v_relay if relay else v_send).at[lane],
             recv_sem=v_recv.at[to, half, block],
             device_id={"fs": mate} if peer is None else {"tp": peer},
             device_id_type=MESH,
@@ -126,9 +122,9 @@
 
     def gain_copy(block, peer, relay=False):
         return pltpu.make_async_remote_copy(
-            src_ref=gain_all.at[block] if relay else gain_rows,
+            src_ref=gain_all.at[block],
             dst_ref=gain_all.at[block],
-            send_sem=g_relay.at[block] if relay else g_send.at[peer],
+            send_sem=g_send,
             recv_sem=g_recv.at[block],
             device_id={"tp": peer},
             device_id_type=MESH,
@@ -144,7 +140,7 @@
         return pltpu.make_async_remote_copy(
             src_ref=source,
             dst_ref=target,
-            send_sem=m_send.at[ffn, number],
+            send_sem=m_send.at[ffn],
             recv_sem=m_recv.at[ffn, number],
             device_id={"fs": mate},
             device_id_type=MESH,
@@ -154,7 +150,7 @@
         return pltpu.make_async_remote_copy(
             src_ref=mate_out.at[ffn, halves[1], :],
             dst_ref=mate_in.at[ffn, tp],
-            send_sem=m_send.at[ffn, tp],
+            send_sem=m_send.at[ffn],
             recv_sem=m_recv.at[ffn, tp],
             device_id={"fs": mate},
             device_id_type=MESH,
@@ -166,7 +162,7 @@
         return pltpu.make_async_remote_copy(
             src_ref=parts.at[lane, block, span, :],
             dst_ref=sums.at[lane, slot, span, :],
-            send_sem=s_send.at[lane, number, block],
+            send_sem=s_send.at[lane],
             recv_sem=s_recv.at[lane, number, slot],
             device_id={"tp": peer},
             device_id_type=MESH,
@@ -232,7 +228,7 @@
         return pltpu.make_async_remote_copy(
             src_ref=own_place(piece) if own else spot,
             dst_ref=spot,
-            send_sem=z_send.at[piece, planes if own and step < 0 else plane],
+            send_sem=z_send.at[piece],
             recv_sem=z_recv.at[piece, plane],
             device_id={"fs": f + step},
             device_id_type=MESH,
@@ -244,7 +240,7 @@
         return pltpu.make_async_remote_copy(
             src_ref=spot,
             dst_ref=spot,
-            send_sem=y_send.at[piece, plane, number],
+            send_sem=y_send.at[piece],
             recv_sem=y_recv.at[piece, plane, there],
             device_id={"grp": other_grps[number]},
             device_id_type=MESH,
@@ -350,7 +346,7 @@
         return [p for p, piece in enumerate(pieces) if piece[0] in numbers]
 
     clock = [0]
-    ahead = 3
+    ahead = 2
     mixer_pieces = of(3, 4, 5)
     early_at = {8 * mixer_pieces[0] // 24 + i: p for i, p in enumerate(mixer_pieces)}
     lag = 1
@@ -386,9 +382,6 @@
     def local_input():
         return pltpu.make_async_copy(inputs, input_all.at[tp], local_sem.at[len(weights)])
 
-    def local_gain():
-        return pltpu.make_async_copy(gain_rows, gain_all.at[tp], local_sem.at[len(weights) + 1])
-
     row_tile = [t for t in (96, 64, 32, 16) if rows % t == 0][0]
 
     def spread(lane, half, with_mate=False):
@@ -534,27 +527,35 @@
     def ffn_lanes(ffn):
         return [ffn * (mates + 1) + slot for slot in range(mates)]
 
+    def project_cross(ffn, slot):
+        lane = ffn_lanes(ffn)[slot]
+        for twin, cross in zip(twins, crosses):
+            product(hidden, down_of, lane, slot, cross)
+            sum_copy(lane, cross, twin, partner).start()
+
+    def project_twin(ffn, slot):
+        lane = ffn_lanes(ffn)[slot]
+        for twin, cross in zip(twins, crosses):
+            product(hidden, down_of, lane, slot, twin)
+            join_cross(lane, twin, cross)
+            if slot > 0:
+                mate_sum_copy(ffn, twin).start()
+            sum_copy(lane, twin, tp, twin, 0).start()
+            if mates == 1:
+                sum_copy(lane, twin, tp, twin, 1).start()
+
+    def project_partner(ffn, slot):
+        lane = ffn_lanes(ffn)[slot]
+        product(hidden, down_of, lane, slot, partner)
+        sum_copy(lane, partner, tp, partner).start()
+
+    def project_own(ffn, slot):
+        product(hidden, down_of, ffn_lanes(ffn)[slot], slot, tp)
+
     def project_ffn(ffn):
-        lanes = ffn_lanes(ffn)
-        order = range(mates - 1, -1, -1)
-        for slot in order:
-            for twin, cross in zip(twins, crosses):
-                product(hidden, down_of, lanes[slot], slot, cross)
-                sum_copy(lanes[slot], cross, twin, partner).start()
-        for slot in order:
-            for twin, cross in zip(twins, crosses):
-                product(hidden, down_of, lanes[slot], slot, twin)
-                join_cross(lanes[slot], twin, cross)
-                if slot > 0:
-                    mate_sum_copy(ffn, twin).start()
-                sum_copy(lanes[slot], twin, tp, twin, 0).start()
-                if mates == 1:
-                    sum_copy(lanes[slot], twin, tp, twin, 1).start()
-        for slot in order:
-            product(hidden, down_of, lanes[slot], slot, partner)
-            sum_copy(lanes[slot], partner, tp, partner).start()
-        for slot in order:
-            product(hidden, down_of, lanes[slot], slot, tp)
+        for stage in (project_cross, project_twin, project_partner, project_own):
+            for slot in range(mates - 1, -1, -1):
+                stage(ffn, slot)
 
     def half_total(lane, half, joined=False):
         total = parts[lane, tp, halves[half], :].astype(F32)
@@ -609,7 +610,11 @@
                 mate_sum_copy(ffn, twin).wait_send()
 
     local_input().start()
-    local_gain().start()
+    row = lax.broadcasted_iota(jnp.int32, (GAIN_ROWS, width), 0)
+    gains = [ref[...].astype(F32) for ref in (first_gain, mixer_gain, second_gain)]
+    gain_all[tp] = jnp.where(
+        row == 0, gains[0], jnp.where(row == 1, gains[1], gains[2])
+    ).astype(BF16)
     for half in range(2):
         spread(0, half)
     for peer in peers:
@@ -621,7 +626,6 @@
     with scope("begin"):
         advance(1)
     local_input().wait()
-    local_gain().wait()
     with scope("input_own"):
         for twin in twins:
             gain_copy(twin, partner).wait_recv()
@@ -752,17 +756,23 @@
         scale_values(2, 0, 2)
     with scope("hidden2_0"):
         hidden_units(0)
+    with scope("project2_0"):
+        project_cross(1, 0)
+        if mates > 1:
+            relay_mate_twins(4)
+        project_partner(1, 0)
+        project_own(1, 0)
+        project_twin(1, 0)
     if mates > 1:
-        with scope("relay4"):
-            relay_mate_twins(4)
-            for piece in of(3, 4, 5):
-                sent(piece)
         with scope("scale4"):
             scale_values(4, 1, 2)
         with scope("hidden2_1"):
             hidden_units(1)
-    with scope("project2"):
-        project_ffn(1)
+        with scope("project2_1"):
+            project_cross(1, 1)
+            project_partner(1, 1)
+            project_twin(1, 1)
+            project_own(1, 1)
     with scope("exchange2"):
         exchange_ffn(1)
     with scope("sent4"):
@@ -770,9 +780,8 @@
         value_sent(2, with_mate=True)
         if mates > 1:
             mate_sent(4)
-        else:
-            for piece in of(3, 4, 5):
-                sent(piece)
+        for piece in of(3, 4, 5):
+            sent(piece)
     with scope("final"):
         for half, span in enumerate(halves):
             out[span, :] = (
@@ -801,13 +810,11 @@
 ):
     rows, width = layer_input.shape
     features = width * tps
-    gains = jnp.concatenate([first_gain, mixer_gain, second_gain], axis=0)
-    gain_rows = jnp.pad(gains, ((0, GAIN_ROWS - 3), (0, 0)))
     units = ffn_gate_w.shape[1]
     channels = pool_in_w.shape[1]
     mates = 2 if planes % 2 == 0 else 1
     fine = max(8 // planes, 1)
-    wanted = (fine, fine, fine, max(fine // 2, 1), fine, max(fine // 2, 1))
+    wanted = (fine, fine, 2 * fine, max(fine // 2, 1), fine, max(fine // 2, 1))
     shards = (ffn_gate_w, ffn_up_w, ffn_down_w, pool_in_w, mixer_gate_w, mixer_out_w)
     talls = [shard.shape[0] // grps for shard in shards]
     talls[2] //= mates
@@ -820,7 +827,7 @@
     return pl.pallas_call(
         functools.partial(layer_kernel, (grps, planes, tps, mates, piece_counts)),
         out_shape=jax.ShapeDtypeStruct((rows, width), BF16),
-        in_specs=[remote] * 8 + [whole] * 2,
+        in_specs=[remote] + [whole] * 3 + [remote] * 6 + [whole] * 2,
         out_specs=whole,
         scratch_shapes=[
             pltpu.VMEM((mates, features, units // mates), BF16),
@@ -842,26 +849,25 @@
             pltpu.VMEM((2, rows, width), BF16),
             pltpu.VMEM((2, tps, rows // 2, width), BF16),
             pltpu.VMEM((2, rows // 2, width), BF16),
-            dma((len(shards) + 2,)),
+            dma((len(shards) + 1,)),
             dma((n, planes)),
             dma((n, planes, max(grps - 1, 1))),
-            dma((n, planes + 1)),
-            dma((n, planes, max(grps - 1, 1))),
-            dma((5, 2, tps + 1)),
-            dma((5, 2, tps, 2)),
+            dma((n,)),
+            dma((n,)),
+            dma((5,)),
+            dma((5,)),
             dma((5, 2, tps)),
+            dma(()),
             dma((tps,)),
-            dma((tps,)),
-            dma((tps,)),
+            dma((lanes,)),
             dma((lanes, 2, tps)),
-            dma((lanes, 2, tps)),
-            dma((2, tps + 1)),
+            dma((2,)),
             dma((2, tps + 1)),
         ],
         compiler_params=pltpu.CompilerParams(
             collective_id=0, has_side_effects=True, vmem_limit_bytes=60 * 1024 * 1024
         ),
-    )(layer_input, gain_rows, *shards, group_mix_w, pool_scale)
+    )(layer_input, first_gain, mixer_gain, second_gain, *shards, group_mix_w, pool_scale)
 
 
 def solution(mesh):

time: 220 us -> 215 us (0.977)
  Pallas kernels: 216 us -> 213 us
    pallas_call x1, Pallas kernels: 216 us -> 213 us  [per_device(): pl.pallas_call(functools.partial(layer_kernel, (grps, planes, tps, mates,...]
where the time goes in v2:
time: 215 us
  Pallas kernels  213 us (99%)
    pallas_call x1, Pallas kernels, per_device(): pl.pallas_call(functools.partial(layer_kernel, (grps, planes, tps, mates,...  213 us

profile of v2, /device:TPU:0, one launch (start us, length us, event | category | flops | bytes accessed | tf_op | source)
XLA Modules:
  0.0 215.1 jit_solution(17202193660664575034)
XLA Ops:
  0.0 213.4 %shard_map.118 = bf16[384,512]{1,0:T(8,128)(2,1)} custom-call(bf16[384,512]{1,0:T(8,128)(2,1)} %inputs.1, bf16[1,512]{1,0:T(2,128)(2,1)} %first_gain.1, bf16[1,512]{1,0:T(2,128)(2,1)} %mixer_gain.1, bf16[1,512]{1,0:T(2,128)(2,1)} %second_gain.1, bf16[512,1536]{1,0:T(8,128)(2,1)} %gate_w.1, bf16[512,1536]{1,0:T(8,128)(2,1)} %up_w.1, ...), custom_call_target="tpu_custom_call" | custom-call | tf_op jit(solution)/shard_map/pallas_call | solution.py:827
  213.4 1.8 copy.14

commit v3 on v2

--- a/solution.py
+++ b/solution.py
@@ -538,10 +538,10 @@
         for twin, cross in zip(twins, crosses):
             product(hidden, down_of, lane, slot, twin)
             join_cross(lane, twin, cross)
-            if slot > 0:
+            if slot > 0 and ffn > 0:
                 mate_sum_copy(ffn, twin).start()
             sum_copy(lane, twin, tp, twin, 0).start()
-            if mates == 1:
+            if mates == 1 or ffn == 0:
                 sum_copy(lane, twin, tp, twin, 1).start()
 
     def project_partner(ffn, slot):
@@ -569,24 +569,32 @@
             total = total + sums[lane, twin, halves[half], :].astype(F32)
         return total
 
-    def exchange_ffn(ffn):
-        lanes = ffn_lanes(ffn)
-        if mates > 1:
-            sum_copy(lanes[1], partner, partner, partner).wait_recv()
-            mate_out[ffn, halves[1], :] = half_total(lanes[1], 1).astype(BF16)
+    def return_half(ffn, half):
+        lane = ffn_lanes(ffn)[1]
+        mate_out[ffn, halves[half], :] = add_twins(lane, half, half_total(lane, half)).astype(BF16)
+        if half == 0:
+            mate_sum_copy(ffn, tp, top=True).start()
+        else:
             own_sum_copy(ffn).start()
+
+    def partner_sums(ffn):
+        for lane in ffn_lanes(ffn):
+            sum_copy(lane, partner, partner, partner).wait_recv()
+
+    def exchange_second():
+        lanes = ffn_lanes(1)
+        partner_sums(1)
+        if mates > 1:
+            mate_out[1, halves[1], :] = half_total(lanes[1], 1).astype(BF16)
+            own_sum_copy(1).start()
             for twin in twins:
-                mate_sum_copy(ffn, twin).wait_recv()
+                mate_sum_copy(1, twin).wait_recv()
                 parts[lanes[0], twin, halves[1], :] = (
                     parts[lanes[0], twin, halves[1], :].astype(F32)
-                    + mate_in[ffn, twin].astype(F32)
+                    + mate_in[1, twin].astype(F32)
                 ).astype(BF16)
                 sum_copy(lanes[0], twin, tp, twin, 1).start()
-            mate_out[ffn, halves[0], :] = add_twins(
-                lanes[1], 0, half_total(lanes[1], 0)
-            ).astype(BF16)
-            mate_sum_copy(ffn, tp, top=True).start()
-        sum_copy(lanes[0], partner, partner, partner).wait_recv()
+            return_half(1, 0)
 
     def ffn_total(ffn, half):
         lane = ffn_lanes(ffn)[0]
@@ -603,10 +611,10 @@
         lanes = ffn_lanes(ffn)
         sum_sent(lanes[0])
         if mates > 1:
-            sum_sent(lanes[1], half_only=0)
+            sum_sent(lanes[1], half_only=0 if ffn else None)
             own_sum_copy(ffn).wait_send()
             mate_sum_copy(ffn, tp, top=True).wait_send()
-            for twin in twins:
+            for twin in twins if ffn else []:
                 mate_sum_copy(ffn, twin).wait_send()
 
     local_input().start()
@@ -672,20 +680,26 @@
         arrive(2)
     with scope("project0"):
         project_ffn(0)
-    with scope("mix_pool"):
-        advance(after(of(3)[-1]))
-    with scope("exchange0"):
-        exchange_ffn(0)
-    with scope("mix_gate"):
-        advance(after(of(4)[0]))
-    with scope("first"):
-        for half, span in enumerate(halves):
+    done = after(len(pieces) - 1)
+    for half in range(2):
+        with scope(f"mix{half}"):
+            advance(min(clock[0] + 1, done))
+        with scope(f"exchange0_{half}"):
+            if half == 0:
+                partner_sums(0)
+            if mates > 1:
+                return_half(0, half)
+    for half, span in enumerate(halves):
+        with scope(f"mix{2 + half}"):
+            if half == 1:
+                advance(min(clock[0] + 1, done))
+        with scope(f"first{half}"):
             value_all[0, tp, span, :] = (
                 input_all[tp, span, :].astype(F32) + 0.5 * ffn_total(0, half)
             ).astype(BF16)
             spread(1, half)
     with scope("mix_rest"):
-        advance(after(len(pieces) - 1))
+        advance(done)
     with scope("sent1"):
         value_sent(0, with_mate=True)
         for peer in peers:
@@ -774,7 +788,7 @@
             project_twin(1, 1)
             project_own(1, 1)
     with scope("exchange2"):
-        exchange_ffn(1)
+        exchange_second()
     with scope("sent4"):
         sum_sent(mates)
         value_sent(2, with_mate=True)

time: 215 us -> 214 us (level)
  no operation moved by 1% of the time
where the time goes in v3:
time: 214 us; the launch traced here: 213 us
  Pallas kernels  211 us (99%)
    pallas_call x1, Pallas kernels, per_device(): pl.pallas_call(functools.partial(layer_kernel, (grps, planes, tps, mates,...  211 us

profile of v3, /device:TPU:0, one launch (start us, length us, event | category | flops | bytes accessed | tf_op | source)
XLA Modules:
  0.0 213.2 jit_solution(14785250973738627745)
XLA Ops:
  0.0 211.5 %shard_map.118 = bf16[384,512]{1,0:T(8,128)(2,1)} custom-call(bf16[384,512]{1,0:T(8,128)(2,1)} %inputs.1, bf16[1,512]{1,0:T(2,128)(2,1)} %first_gain.1, bf16[1,512]{1,0:T(2,128)(2,1)} %mixer_gain.1, bf16[1,512]{1,0:T(2,128)(2,1)} %second_gain.1, bf16[512,1536]{1,0:T(8,128)(2,1)} %gate_w.1, bf16[512,1536]{1,0:T(8,128)(2,1)} %up_w.1, ...), custom_call_target="tpu_custom_call" | custom-call | tf_op jit(solution)/shard_map/pallas_call | solution.py:841
  211.5 1.8 copy.14
